TPU v7x, 512 devices: a whole 4x8x8 slice. The times are simulated.
512 devices in a mesh: sp: 64 (over z, y), fs: 4 (over x), tp: 2 (over core).
Axes of the slice: x: 4, y: 8, z: 8, core: 2. Of those that a mesh axis runs over, the one named last changes fastest.
Arguments:
- tokens: bfloat16 [32768, 2048], P(('fs', 'sp')), may hold values from -6 to 6
- in_gain: float32 [2048], replicated, may hold values from 0.1 to 1.9
- query_weight: bfloat16 [2048, 512], P(None, ('tp', 'fs')), may hold values from -0.17291713 to 0.17291713
- key_weight: bfloat16 [2048, 512], P(None, ('tp', 'fs')), may hold values from -0.17291713 to 0.17291713
- value_weight: bfloat16 [2048, 512], P(None, ('tp', 'fs')), may hold values from -0.125 to 0.125
- rec_query_weight: bfloat16 [2048, 512], P(None, ('tp', 'fs')), may hold values from -0.125 to 0.125
- rec_forget_weight: bfloat16 [2048, 512], P(None, ('tp', 'fs')), may hold values from -0.125 to 0.125
- rec_input_weight: bfloat16 [2048, 512], P(None, ('tp', 'fs')), may hold values from -0.125 to 0.125
- mix_lambda: float32 [4], P('tp'), may hold values from 0.3 to 0.8
- lower_bound: float32 [4, 128], P('tp'), may hold values from 0.9 to 0.9999695
- forget_scale: float32 [32768], P(('fs', 'sp')), may hold values from 0.35 to 24576
- att_gain: float32 [128], replicated, may hold values from 0.1 to 1.9
- recurrence_gain: float32 [128], replicated, may hold values from 0.1 to 1.9
- att_out_weight: bfloat16 [512, 2048], P('tp'), may hold values from -0.1875 to 0.1875
- rec_out_weight: bfloat16 [512, 2048], P('tp'), may hold values from -0.1875 to 0.1875
Outputs:
- mixed_out: bfloat16 [32768, 2048], P(('fs', 'sp'))
- log_weight_sum: float32 [4, 32768], P('tp', ('fs', 'sp'))
All inputs are finite; a program needn't handle non-finite values.
Results may differ from a plain program's by a relative error of at most 0.012.
Values may be sent and summed in bfloat16 or wider, within the bound.
A program may use at most 128 MiB of HBM per device.

v0:
```python
import jax
import jax.numpy as jnp
from jax import lax
from jax.sharding import Mesh
from jax.sharding import PartitionSpec as P

DK = 64
DV = 128
BLK = 64
SP = ("sp_0", "sp_1")
FS_SP = ("fs", "sp_0", "sp_1")
EPS = 1e-06
NEG = -1e30


def in_one_piece(arrays, axis, dim, along):
    widths = [a.shape[along] for a in arrays]
    both = jnp.concatenate(arrays, axis=along)
    filled = lax.all_gather(both, axis, axis=dim, tiled=True)
    return tuple(jnp.split(filled, [sum(widths[:k]) for k in range(1, len(widths))], axis=along))


def nothing_yet(x, identity):
    return jax.tree.map(
        lambda part, zero: jnp.zeros_like(part) + jnp.asarray(zero, part.dtype), x, identity
    )


def entering(x, axes, combine, identity):
    before = start = nothing_yet(x, identity)
    running = x
    for axis in reversed(axes):
        peers, here = (lax.axis_size(axis), lax.axis_index(axis))
        pieces = jax.tree.map(lambda part: lax.all_gather(part, axis), running)
        inside, running = (start, start)
        for k in range(peers):
            passed = k < here
            running = combine(running, jax.tree.map(lambda part: part[k], pieces))
            inside = jax.tree.map(lambda new, old: jnp.where(passed, new, old), running, inside)
        before = combine(inside, before)
    return before


def copy_for_each(x, axis):
    peers = lax.axis_size(axis)
    return lax.all_to_all(jnp.broadcast_to(x[None], (peers, *x.shape)), axis, 0, 0, tiled=True)


def taken_together(x, axis):
    return copy_for_each(x, axis).astype(jnp.float32).sum(axis=0)


def norm_rows(values, gain):
    return values * lax.rsqrt(jnp.mean(values * values, axis=-1, keepdims=True) + EPS) * gain


def block_recurrence(queries, key_in, value_in, log_forget):
    head_count, row_count, key_width = queries.shape
    block_count = row_count // BLK

    def to_blocks(array_in):
        return array_in.reshape(head_count, block_count, BLK, array_in.shape[-1]).transpose(
            1, 0, 2, 3
        )

    causal = jnp.tril(jnp.ones((BLK, BLK), bool))

    def advance(passed_state, inputs):
        query_block, key_block, value_block, l_blk = inputs
        accumulator_sum = jnp.cumsum(l_blk, axis=1)
        cross_block_output = jnp.einsum(
            "sre,sei->sri",
            query_block * jnp.exp(accumulator_sum),
            passed_state,
            precision=lax.Precision.HIGHEST,
        )
        spread = accumulator_sum[:, :, None, :] - accumulator_sum[:, None, :, :]
        decay = jnp.exp(jnp.where(causal[None, :, :, None], spread, -jnp.inf))
        scores = jnp.einsum(
            "htk,htsk,hsk->hts", query_block, decay, key_block, precision=lax.Precision.HIGHEST
        )
        result = cross_block_output + jnp.einsum(
            "hts,hsv->htv", scores, value_block, precision=lax.Precision.HIGHEST
        )
        final_log_sum = accumulator_sum[:, -1:, :]
        updated_state = jnp.exp(final_log_sum[:, 0, :])[:, :, None] * passed_state + jnp.einsum(
            "plf,plt->pft",
            key_block * jnp.exp(final_log_sum - accumulator_sum),
            value_block,
            precision=lax.Precision.HIGHEST,
        )
        return (updated_state, result)

    begin_state = jnp.zeros((head_count, key_width, value_in.shape[-1]), jnp.float32)
    end_state, results = lax.scan(
        advance,
        begin_state,
        (to_blocks(queries), to_blocks(key_in), to_blocks(value_in), to_blocks(log_forget)),
    )
    return (
        end_state,
        results.transpose(1, 0, 2, 3).reshape(head_count, row_count, value_in.shape[-1]),
    )


def attend(online, queries, pair_keys, pair_values, allowed):
    running_max, weight_sum, numer_sum = online
    local_heads = numer_sum.shape[0]
    key_rows = pair_keys.shape[0]
    key_heads = pair_keys.reshape(key_rows, local_heads, 2, DK).transpose(1, 2, 0, 3)
    head_values = pair_values.reshape(key_rows, local_heads, DV).transpose(1, 0, 2)
    scores = jnp.einsum(
        "hmqd,hmkd->hmqk", queries, key_heads, preferred_element_type=jnp.float32
    ) * DK ** (-0.5)
    scores = jnp.where(allowed, scores, NEG)
    highest = jnp.maximum(running_max, jnp.max(scores, axis=-1))
    weights = jnp.exp(scores - highest[..., None])
    weight_sum = jnp.sum(weights, axis=-1)
    numer_sum = jnp.einsum(
        "itap,ipn->itan",
        weights.astype(jnp.bfloat16),
        head_values,
        preferred_element_type=jnp.float32,
    )
    return (highest, weight_sum, numer_sum)


def on_device(
    tokens,
    in_gain,
    query_weight,
    key_weight,
    value_weight,
    rec_query_weight,
    rec_forget_weight,
    rec_input_weight,
    mix_lambda,
    lower_bound,
    forget_scale,
    att_gain,
    recurrence_gain,
    att_out_weight,
    rec_out_weight,
):
    normed = norm_rows(tokens.astype(jnp.float32), in_gain).astype(jnp.bfloat16)
    row_count = normed.shape[0]
    stacked = jnp.stack(
        [
            query_weight,
            key_weight,
            value_weight,
            rec_query_weight,
            rec_forget_weight,
            rec_input_weight,
        ],
        axis=1,
    )
    projected = jnp.einsum(
        "rd,dnc->rnc",
        normed,
        lax.all_gather(stacked, "fs", axis=2, tiled=True),
        preferred_element_type=jnp.float32,
    ).astype(jnp.bfloat16)
    local_heads = projected.shape[2] // DV
    position = lax.axis_index(SP)
    query_pos = position * row_count + jnp.arange(row_count)
    queries = projected[:, 0].reshape(row_count, local_heads, 2, DK).transpose(1, 2, 0, 3)
    online = (
        jnp.full((local_heads, 2, row_count), NEG, jnp.float32),
        jnp.zeros((local_heads, 2, row_count), jnp.float32),
        jnp.zeros((local_heads, 2, row_count, DV), jnp.float32),
    )
    pair_keys, pair_values = in_one_piece((projected[:, 1], projected[:, 2]), SP, 0, 1)
    key_pos = jnp.arange(pair_keys.shape[0])
    allowed = query_pos[:, None] >= key_pos[None, :]
    online = lax.cond(
        jnp.int32(0) <= query_pos[-1],
        lambda state: attend(state, queries, pair_keys, pair_values, allowed),
        lambda state: state,
        online,
    )
    running_max, weight_sum, numer_sum = online
    mixed_heads = (
        numer_sum[:, 0] / weight_sum[:, 0, :, None]
        - mix_lambda[:, None, None] * numer_sum[:, 1] / weight_sum[:, 1, :, None]
    )
    att_heads = (norm_rows(mixed_heads, att_gain) * 0.8).astype(jnp.bfloat16)
    att_rows = att_heads.transpose(1, 0, 2).reshape(row_count, local_heads * DV)
    log_weight_sum = running_max[:, 0] + jnp.log(weight_sum[:, 0])

    def heads_first(array_in):
        return array_in.reshape(row_count, local_heads, DV).transpose(1, 0, 2).astype(jnp.float32)

    recurrent_queries = heads_first(projected[:, 3])
    lower_edge = lower_bound[:, None, :]
    forget = lower_edge + (1.0 - lower_edge) * jax.nn.sigmoid(heads_first(projected[:, 4]))
    log_forget = forget_scale[None, :, None] * jnp.log(forget)
    key_in = 1.0 - jnp.exp(log_forget)
    end_state, local_result = block_recurrence(
        recurrent_queries, key_in, heads_first(projected[:, 5]), log_forget
    )
    running_state = jnp.cumsum(log_forget, axis=1)
    carry_rate = jnp.exp(running_state[:, -1, :])

    def combine(earlier, later):
        return (later[0] * earlier[0], later[0][..., None] * earlier[1] + later[1])

    identity = (jnp.ones_like(carry_rate), jnp.zeros_like(end_state))
    _, incoming_state = entering((carry_rate, end_state), SP, combine, identity)
    combined = local_result + jnp.einsum(
        "zed,zdp->zep",
        recurrent_queries * jnp.exp(running_state),
        incoming_state,
        precision=lax.Precision.HIGHEST,
    )
    rec_heads = norm_rows(combined, recurrence_gain).astype(jnp.bfloat16)
    rec_rows = rec_heads.transpose(1, 0, 2).reshape(row_count, local_heads * DV)
    partial_value = jnp.dot(att_rows, att_out_weight, preferred_element_type=jnp.float32) + jnp.dot(
        rec_rows, rec_out_weight, preferred_element_type=jnp.float32
    )
    mixed_out = (
        taken_together(partial_value.astype(jnp.bfloat16), "tp")
        .astype(jnp.float32)
        .astype(jnp.bfloat16)
    )
    return (mixed_out, log_weight_sum)


def solution(mesh):
    finer = Mesh(
        mesh.devices.reshape(8, 8, mesh.shape["fs"], mesh.shape["tp"]), ("sp_0", "sp_1", "fs", "tp")
    )
    placed = (
        P(FS_SP, None),
        P(),
        P(None, ("tp", "fs")),
        P(None, ("tp", "fs")),
        P(None, ("tp", "fs")),
        P(None, ("tp", "fs")),
        P(None, ("tp", "fs")),
        P(None, ("tp", "fs")),
        P("tp"),
        P("tp", None),
        P(FS_SP),
        P(),
        P(),
        P("tp", None),
        P("tp", None),
    )
    return jax.shard_map(
        on_device,
        mesh=finer,
        in_specs=placed,
        out_specs=(P(FS_SP, None), P("tp", FS_SP)),
        check_vma=False,
    )
```

profile of v0, /device:TPU:1, one launch (start us, length us, event | category | flops | bytes accessed | tf_op | source)
XLA Modules:
  0.0 367.2 jit_solution(1742700413866512903)
XLA Ops:
  7.3 1.1 bitcast_dynamic-update-slice_fusion.5
  8.3 1.0 bitcast_dynamic-update-slice_fusion.4
  13.2 1.1 copy-done.2
  14.7 76.1 %all-gather.7.cloned.1.call-done = bf16[2048,6,256]{0,2,1:T(8,128)(2,1)} async-done(((bf16[2048,6,64]{0,2,1:T(8,128)(2,1)}), bf16[2048,6,256]{0,2,1:T(8,128)(2,1)}) %all-gather.7.cloned.1.call-update) | async-done | bytes 6291472 | tf_op jit(solution)/shard_map/all_gather | solution.py:161
  90.8 5.0 %convolution_convert_fusion = bf16[128,6,256]{2,0,1:T(8,128)(2,1)S(1)} fusion(bf16[2048,6,256]{0,2,1:T(8,128)(2,1)} %all-gather.7.cloned.1.call-done, bf16[128,2048]{1,0:T(8,128)(2,1)S(1)} %copy-done.3, f32[2048]{0:T(1024)S(1)} %copy-done.5, f32[128]{0:T(128)S(1)} %add_rsqrt_fusion.2), kind=kOutput, calls=%fused_computation.55 | convolution fusion | flops 806551552 | bytes 7217664 | tf_op jit(solution)/shard_map/rd,dnc->rnc/dot_general | solution.py:158
  96.3 16.1 %while.13 = (s32[]{:T(128)}, f32[2,128,128]{2,1,0:T(8,128)S(1)}, f32[2,2,64,128]{3,2,0,1:T(8,128)S(1)}, f32[2,2,64,128]{3,2,0,1:T(8,128)S(1)}, f32[2,2,64,128]{3...) while((s32[]{:T(128)}, f32[2,128,128]{2,1,0:T(8,128)S(1)}, ...), condition=%wide.region_8.9_spmd.clone, body=%wide.region_6.8_spmd.clone.sunk | while | flops 79876096 | bytes 1819267 | solution.py:95
  96.5 6.9 %fusion.202 = f32[2,64,1,64]{3,2,1,0:T(1,128)S(1)} fusion(f32[2,64,128,1]{2,3,1,0:T(1,128)S(1)} %bitcast.358, f32[2,64,128]{2,1,0:T(8,128)S(1)} %get-tuple-element.238, f32[2,64,128]{2,1,0:T(8,128)S(1)} %reduce_window_sum.25, pred[64,64]{1,0:T(8,128)(4,1)S(1)} %iota_compare_fusion.2), kind=kOutput, calls=%fused_computation.14.clone.1 | convolution fusion | flops 15728640 | bytes 233472 | tf_op jit(solution)/shard_map/while/body/eval_jaxpr/htk,htsk,hsk->hts/dot_general | solution.py:79
  104.5 6.9 %fusion.202 = f32[2,64,1,64]{3,2,1,0:T(1,128)S(1)} fusion(f32[2,64,128,1]{2,3,1,0:T(1,128)S(1)} %bitcast.358, f32[2,64,128]{2,1,0:T(8,128)S(1)} %get-tuple-element.238, f32[2,64,128]{2,1,0:T(8,128)S(1)} %reduce_window_sum.25, pred[64,64]{1,0:T(8,128)(4,1)S(1)} %iota_compare_fusion.2), kind=kOutput, calls=%fused_computation.14.clone.1 | convolution fusion | flops 15728640 | bytes 233472 | tf_op jit(solution)/shard_map/while/body/eval_jaxpr/htk,htsk,hsk->hts/dot_general | solution.py:79
  113.3 12.4 %all-gather = f32[16,1,128]{2,1,0:T(1,128)S(1)} all-gather(f32[2,1,128]{2,1,0:T(1,128)S(1)} %slice_exponential_fusion), channel_id=2, replica_groups=mesh['sp_0'=8,'sp_1'=8,'fs'=4,'tp'=2] {'sp_1'}, dimensions={0}, use_global_device_ids=true | all-gather | bytes 9216 | tf_op jit(solution)/shard_map/all_gather | solution.py:34
  125.7 24.3 %all-gather.13.cloned.1.call-done = f32[16,128,128]{2,1,0:T(8,128)} async-done(((f32[2,128,128]{2,1,0:T(8,128)}), f32[16,128,128]{2,1,0:T(8,128)}) %all-gather.13.cloned.1.call-update) | async-done | bytes 1048592 | tf_op jit(solution)/shard_map/all_gather | solution.py:34
  150.0 2.3 bitcast_add_fusion
  154.4 13.5 %all_gather.27 = f32[8,2,128]{2,1,0:T(2,128)S(1)} all-gather(f32[1,2,128]{2,1,0:T(2,128)S(1)} %get-tuple-element.183), channel_id=1, replica_groups=mesh['sp_0'=8,'sp_1'=8,'fs'=4,'tp'=2] {'sp_0'}, dimensions={0}, use_global_device_ids=true | all-gather | bytes 9216 | tf_op jit(solution)/shard_map/all_gather | solution.py:34
  168.0 25.6 %all-gather.11.cloned.1.call-done = f32[8,2,128,128]{3,2,1,0:T(8,128)} async-done(((f32[1,2,128,128]{3,2,1,0:T(8,128)}), f32[8,2,128,128]{3,2,1,0:T(8,128)}) %all-gather.11.cloned.1.call-update) | async-done | bytes 1048592 | tf_op jit(solution)/shard_map/all_gather | solution.py:34
  193.5 2.6 multiply_reduce_fusion
  196.3 102.3 %all-gather.9.cloned.1.call-done = bf16[8192,512]{1,0:T(8,128)(2,1)} async-done(((bf16[128,512]{1,0:T(8,128)(2,1)}), bf16[8192,512]{1,0:T(8,128)(2,1)}) %all-gather.9.cloned.1.call-update) | async-done | bytes 8388624 | tf_op jit(solution)/shard_map/all_gather | solution.py:19
  299.0 53.7 %conditional.1 = (f32[2,2,128]{2,1,0:T(2,128)S(1)}, f32[2,2,128,128]{3,2,1,0:T(8,128)S(1)}, f32[2,128]{1,0:T(2,128)S(1)}) conditional(s32[]{:T(128)} %bitcast.8, () %tuple.22, (s32[]{:T(128)}, s32[128,1]{0,1:T(1,128)S(1)}, s32[128,8192]{1,0:T(8,128)S(1)}, bf16[8192,512]{1,0:T(8,128)(2,1)}, bf16[2,2,128,64]{2,3,1,0:T(8,128)(2,1)S(1)}) %tuple.88), branch_computations={%region_1.0_spmd, %region_2.5_spmd} | conditional | flops 1657798272 | bytes 109395480 | solution.py:176
  299.9 11.9 %copy.86 = bf16[8192,512]{0,1:T(8,128)(2,1)} copy(bf16[8192,512]{1,0:T(8,128)(2,1)} %get-tuple-element.135) | data formatting | bytes 16777216 | tf_op jit(solution)/shard_map
  311.8 5.9 %fusion.173 = (bf16[8192,256]{0,1:T(8,128)(2,1)}, bf16[8192,256]{0,1:T(8,128)(2,1)}) fusion(bf16[8192,512]{0,1:T(8,128)(2,1)} %copy.86), kind=kLoop, calls=%fused_computation.242 | loop fusion | bytes 16777216 | tf_op jit(solution)/shard_map/split | solution.py:20
  317.8 6.3 %copy.84 = bf16[8192,2,128]{2,0,1:T(8,128)(2,1)} copy(bf16[8192,2,128]{0,2,1:T(8,128)(2,1)} %bitcast.357) | data formatting | bytes 8388608 | tf_op jit(solution)/shard_map/cond/branch_1_fun/reshape | solution.py:111
  324.1 11.2 %fusion.2 = (f32[2,2,128]{2,1,0:T(2,128)S(1)}, f32[2,2,128,8192]{3,2,1,0:T(8,128)}) fusion(pred[128,8192]{1,0:T(8,128)(4,1)S(1)} %broadcast_compare_fusion, bf16[2,2,128,64]{2,3,1,0:T(8,128)(2,1)S(1)} %get-tuple-element.54, bf16[2,2,8192,64]{2,3,1,0:T(8,128)(2,1)} %bitcast.361), kind=kOutput, calls=%fused_computation.3 | convolution fusion | flops 549453312 | bytes 22087680 | tf_op jit(solution)/shard_map/cond/branch_1_fun/hmqd,hmkd->hmqk/dot_general | solution.py:112
  335.3 9.3 %fusion.5 = f32[2,2,128,128]{3,2,1,0:T(8,128)S(1)} fusion(f32[2,2,128,8192]{3,2,1,0:T(8,128)} %get-tuple-element.165, f32[2,2,128]{2,1,0:T(2,128)S(1)} %broadcast_maximum_fusion, pred[128,8192]{1,0:T(8,128)(4,1)S(1)} %broadcast_compare_fusion, bf16[8192,2,128]{2,0,1:T(8,128)(2,1)} %copy.84), kind=kOutput, calls=%fused_computation.6 | convolution fusion | flops 1090519040 | bytes 22284288 | tf_op jit(solution)/shard_map/cond/branch_1_fun/itap,ipn->itan/dot_general | solution.py:119
  344.6 8.1 %fusion.4 = f32[2,2,128]{2,1,0:T(2,128)S(1)} fusion(f32[2,2,128,8192]{3,2,1,0:T(8,128)} %get-tuple-element.165, f32[2,2,128]{2,1,0:T(2,128)S(1)} %broadcast_maximum_fusion, pred[128,8192]{1,0:T(8,128)(4,1)S(1)} %broadcast_compare_fusion), kind=kLoop, calls=%fused_computation.5 | loop fusion | flops 16776704 | bytes 17829888 | tf_op jit(solution)/shard_map/cond/branch_1_fun/reduce_sum | solution.py:118
  354.5 5.1 %all_to_all.5 = bf16[2,128,2048]{2,1,0:T(8,128)(2,1)S(1)} all-to-all(bf16[2,128,2048]{2,1,0:T(8,128)(2,1)S(1)} %broadcast_in_dim.46), channel_id=1, replica_groups=mesh['sp_0'=8,'sp_1'=8,'fs'=4,'tp'=2] {'tp'}, dimensions={0} | all-to-all | bytes 2097152 | tf_op jit(solution)/shard_map/all_to_all | solution.py:46
  359.6 1.1 reduce_sum.51
  (95 shorter events, 12.0 us)
Async XLA Ops:
  7.2 346.5 %copy-start = (bf16[256,2048]{1,0:T(8,128)(2,1)S(1)}, bf16[256,2048]{1,0:T(8,128)(2,1)}, u32[]{:S(2)}) copy-start(bf16[256,2048]{1,0:T(8,128)(2,1)} %param.32) | copy-start | bytes 3145732
  7.2 7.3 %copy-start.3 = (bf16[128,2048]{1,0:T(8,128)(2,1)S(1)}, bf16[128,2048]{1,0:T(8,128)(2,1)}, u32[]{:S(2)}) copy-start(bf16[128,2048]{1,0:T(8,128)(2,1)} %param.19) | copy-start | bytes 1572868
  7.2 7.5 %copy-start.6 = (f32[2,128]{1,0:T(2,128)S(1)}, f32[2,128]{1,0:T(2,128)}, u32[]{:S(2)}) copy-start(f32[2,128]{1,0:T(2,128)} %param.28) | copy-start | bytes 3076
  7.2 83.6 %copy-start.5 = (f32[2048]{0:T(1024)S(1)}, f32[2048]{0:T(1024)}, u32[]{:S(2)}) copy-start(f32[2048]{0:T(1024)} %param.20) | copy-start | bytes 24580
  7.2 83.6 %all-gather.7.cloned.1.call-start = ((), (), s32[]{:S(2)}) async-start(), calls=%async_computation.1 | async-start | bytes 7864320 | tf_op jit(solution)/shard_map/all_gather | solution.py:161
  13.2 1.1 copy-start.2
  14.4 135.6 %all-gather.13.cloned.1.call-start = ((), (), s32[]{:S(2)}) async-start(), calls=%async_computation.4 | async-start | bytes 1179648 | tf_op jit(solution)/shard_map/all_gather | solution.py:34
  14.7 81.5 %copy-start.7 = (f32[128]{0:T(128)S(1)}, f32[128]{0:T(128)}, u32[]{:S(2)}) copy-start(f32[128]{0:T(128)} %param.29) | copy-start | bytes 1540
  112.4 0.7 copy-start.1
  112.4 83.8 %copy-start.8 = (f32[128]{0:T(128)S(1)}, f32[128]{0:T(128)}, u32[]{:S(2)}) copy-start(f32[128]{0:T(128)} %param.31) | copy-start | bytes 1540
  113.0 80.5 %all-gather.11.cloned.1.call-start = ((), (), s32[]{:S(2)}) async-start(), calls=%async_computation.3 | async-start | bytes 1179648 | tf_op jit(solution)/shard_map/all_gather | solution.py:34
  152.3 146.3 %all-gather.9.cloned.1.call-start = ((), (), s32[]{:S(2)}) async-start(), calls=%async_computation.2 | async-start | bytes 8519680 | tf_op jit(solution)/shard_map/all_gather | solution.py:19
  299.0 54.5 %copy-start.9 = (f32[2]{0:T(128)S(1)}, f32[2]{0:T(128)}, u32[]{:S(2)}) copy-start(f32[2]{0:T(128)} %param.27) | copy-start | bytes 28
  299.0 54.6 %copy-start.10 = (f32[128]{0:T(128)S(1)}, f32[128]{0:T(128)}, u32[]{:S(2)}) copy-start(f32[128]{0:T(128)} %param.30) | copy-start | bytes 1540
  299.0 55.0 %copy-start.4 = (bf16[256,2048]{1,0:T(8,128)(2,1)S(1)}, bf16[256,2048]{1,0:T(8,128)(2,1)}, u32[]{:S(2)}) copy-start(bf16[256,2048]{1,0:T(8,128)(2,1)} %param.33) | copy-start | bytes 3145732
Sparse Core Ops, SparseCore 0:
  14.5 76.2 all-gather.6
  113.2 36.8 all-gather.12
  152.4 41.0 all-gather.10
  197.0 101.4 all-gather.8
where the time goes:
time: 368 us; the launch traced here: 367 us
  waiting for transfers between devices  228 us (62%)
  matrix products  44.4 us (12%)
  local copies, waits for them, and re-layouts  33.7 us (9%)
  blocking collectives  31 us (8%)
  between operations  14.8 us (4%)
  other arithmetic  14.5 us (4%)
    all_gather x1, waiting for transfers between devices, in_one_piece(): filled = lax.all_gather(both, axis, axis=dim, tiled=True)  102 us
    all_gather x1, waiting for transfers between devices, on_device(): lax.all_gather(stacked, 'fs', axis=2, tiled=True)  76.1 us
    all_gather x2, waiting for transfers between devices, entering(): pieces = jax.tree.map(lambda part: lax.all_gather(part, axis), running)  49.9 us
    all_gather x2, blocking collectives, entering(): pieces = jax.tree.map(lambda part: lax.all_gather(part, axis), running)  25.9 us
    dot_general x2, matrix products, advance(): jnp.einsum('htk,htsk,hsk->hts', query_block, decay, key_block, precision=...  13.9 us
    another operation x1, local copies, waits for them, and re-layouts  11.9 us
    dot_general x1, matrix products, attend(): jnp.einsum('hmqd,hmkd->hmqk', queries, key_heads, preferred_element_type=...  11.2 us
    dot_general x1, matrix products, attend(): jnp.einsum('itap,ipn->itan', weights.astype(jnp.bfloat16), head_values, p...  9.28 us
  transfers between devices with their start and end apart: 4, of which 4 were waited for; matrix products, arithmetic and copies ran while one was open for 1% of the time, Pallas kernels for 0%

commit v1 on v0

--- a/solution.py
+++ b/solution.py
@@ -11,6 +11,11 @@
 FS_SP = ("fs", "sp_0", "sp_1")
 EPS = 1e-06
 NEG = -1e30
+
+
+def gather_from_all(value, axis, dim):
+    copies = jnp.concatenate([value] * lax.axis_size(axis), axis=dim)
+    return lax.all_to_all(copies, axis, dim, dim, tiled=True)
 
 
 def in_one_piece(arrays, axis, dim, along):
@@ -156,10 +161,7 @@
         axis=1,
     )
     projected = jnp.einsum(
-        "rd,dnc->rnc",
-        normed,
-        lax.all_gather(stacked, "fs", axis=2, tiled=True),
-        preferred_element_type=jnp.float32,
+        "rd,dnc->rnc", normed, gather_from_all(stacked, "fs", 2), preferred_element_type=jnp.float32
     ).astype(jnp.bfloat16)
     local_heads = projected.shape[2] // DV
     position = lax.axis_index(SP)

time: 368 us -> 403 us (1.095)
  waiting for transfers between devices: 228 us -> 242 us
  blocking collectives: 31 us -> 37.7 us
  starting transfers between devices: 0.16 us -> 6.07 us
  local copies, waits for them, and re-layouts: 33.7 us -> 39.5 us
    all_to_all x0 -> x1, waiting for transfers between devices: none -> 87.8 us  [gather_from_all(): return lax.all_to_all(copies, axis, dim, dim, tiled=True)]
    all_gather x1 -> x0, waiting for transfers between devices: 76.1 us -> none  [on_device(): lax.all_gather(stacked, 'fs', axis=2, tiled=True)]
    concatenate x0 -> x1, local copies, waits for them, and re-layouts: none -> 6.87 us  [gather_from_all(): copies = jnp.concatenate([value] * lax.axis_size(axis), axis=dim)]
    all_gather x2, blocking collectives: 25.9 us -> 32.5 us  [entering(): pieces = jax.tree.map(lambda part: lax.all_gather(part, axis), running)]
    all_to_all x0 -> x1, starting transfers between devices: none -> 5.77 us  [gather_from_all(): return lax.all_to_all(copies, axis, dim, dim, tiled=True)]
where the time goes in v1:
time: 403 us; the launch traced here: 402 us
  waiting for transfers between devices  242 us (60%)
  matrix products  46.7 us (12%)
  local copies, waits for them, and re-layouts  39.5 us (10%)
  blocking collectives  37.7 us (9%)
  other arithmetic  15.2 us (4%)
  between operations  14.7 us (4%)
  starting transfers between devices  6.07 us (2%)
    all_gather x1, waiting for transfers between devices, in_one_piece(): filled = lax.all_gather(both, axis, axis=dim, tiled=True)  102 us
    all_to_all x1, waiting for transfers between devices, gather_from_all(): return lax.all_to_all(copies, axis, dim, dim, tiled=True)  87.8 us
    all_gather x2, waiting for transfers between devices, entering(): pieces = jax.tree.map(lambda part: lax.all_gather(part, axis), running)  51.8 us
    all_gather x2, blocking collectives, entering(): pieces = jax.tree.map(lambda part: lax.all_gather(part, axis), running)  32.5 us
    dot_general x2, matrix products, advance(): jnp.einsum('htk,htsk,hsk->hts', query_block, decay, key_block, precision=...  13.9 us
    another operation x1, local copies, waits for them, and re-layouts  12 us
    dot_general x1, matrix products, attend(): jnp.einsum('hmqd,hmkd->hmqk', queries, key_heads, preferred_element_type=...  11.2 us
    dot_general x1, matrix products, attend(): jnp.einsum('itap,ipn->itan', weights.astype(jnp.bfloat16), head_values, p...  9.29 us
  transfers between devices with their start and end apart: 4, of which 4 were waited for; matrix products, arithmetic and copies ran while one was open for 1% of the time, Pallas kernels for 0%

profile of v1, /device:TPU:1, one launch (start us, length us, event | category | flops | bytes accessed | tf_op | source)
XLA Modules:
  0.0 402.2 jit_solution(13919195507270002177)
XLA Ops:
  7.2 1.1 bitcast_dynamic-update-slice_fusion.5
  13.9 6.9 %copy.124 = bf16[2048,6,256]{0,1,2:T(8,128)(2,1)} copy(bf16[2048,6,256]{0,2,1:T(8,128)(2,1)S(1)} %pad_maximum_fusion) | data formatting | bytes 12582912 | tf_op jit(solution)/shard_map/concatenate | solution.py:17
  20.8 5.8 %all-to-all-start = ((bf16[2048,6,256]{0,1,2:T(8,128)(2,1)}), bf16[2048,6,256]{0,1,2:T(8,128)(2,1)}, u32[]{:S(2)}, u32[]{:S(2)}) async-start(bf16[2048,6,256]{0,1,2:T(8,128)(2,1)} %copy.124), calls=%async_computation | async-start | bytes 16777216 | tf_op jit(solution)/shard_map/all_to_all | solution.py:18
  27.0 87.8 %all-to-all-done = bf16[2048,6,256]{0,1,2:T(8,128)(2,1)} async-done(((bf16[2048,6,256]{0,1,2:T(8,128)(2,1)}), bf16[2048,6,256]{0,1,2:T(8,128)(2,1)}, u32[]{:S(2)}, u32[]{:S(2)}) %all-to-all-start) | async-done | bytes 6291488 | tf_op jit(solution)/shard_map/all_to_all | solution.py:18
  114.8 7.3 %fusion.44 = bf16[128,6,256]{2,0,1:T(8,128)(2,1)S(1)} fusion(bf16[2048,6,256]{0,1,2:T(8,128)(2,1)} %all-to-all-done, bf16[128,2048]{1,0:T(8,128)(2,1)S(1)} %copy-done.3, f32[2048]{0:T(1024)S(1)} %copy-done.9, f32[128]{0:T(128)S(1)} %add_rsqrt_fusion.2), kind=kOutput, calls=%fused_computation.58 | convolution fusion | flops 806551552 | bytes 7217664 | tf_op jit(solution)/shard_map/rd,dnc->rnc/dot_general | solution.py:163
  122.6 16.1 %while.13 = (s32[]{:T(128)}, f32[2,128,128]{2,1,0:T(8,128)S(1)}, f32[2,2,64,128]{3,2,0,1:T(8,128)S(1)}, f32[2,2,64,128]{3,2,0,1:T(8,128)S(1)}, f32[2,2,64,128]{3...) while((s32[]{:T(128)}, f32[2,128,128]{2,1,0:T(8,128)S(1)}, ...), condition=%wide.region_8.9_spmd.clone, body=%wide.region_6.8_spmd.clone.sunk | while | flops 79876096 | bytes 1819267 | solution.py:100
  122.8 6.9 %fusion.206 = f32[2,64,1,64]{3,2,1,0:T(1,128)S(1)} fusion(f32[2,64,128,1]{2,3,1,0:T(1,128)S(1)} %bitcast.357, f32[2,64,128]{2,1,0:T(8,128)S(1)} %get-tuple-element.250, f32[2,64,128]{2,1,0:T(8,128)S(1)} %reduce_window_sum.25, pred[64,64]{1,0:T(8,128)(4,1)S(1)} %iota_compare_fusion.2), kind=kOutput, calls=%fused_computation.14.clone.1 | convolution fusion | flops 15728640 | bytes 233472 | tf_op jit(solution)/shard_map/while/body/eval_jaxpr/htk,htsk,hsk->hts/dot_general | solution.py:84
  130.8 6.9 %fusion.206 = f32[2,64,1,64]{3,2,1,0:T(1,128)S(1)} fusion(f32[2,64,128,1]{2,3,1,0:T(1,128)S(1)} %bitcast.357, f32[2,64,128]{2,1,0:T(8,128)S(1)} %get-tuple-element.250, f32[2,64,128]{2,1,0:T(8,128)S(1)} %reduce_window_sum.25, pred[64,64]{1,0:T(8,128)(4,1)S(1)} %iota_compare_fusion.2), kind=kOutput, calls=%fused_computation.14.clone.1 | convolution fusion | flops 15728640 | bytes 233472 | tf_op jit(solution)/shard_map/while/body/eval_jaxpr/htk,htsk,hsk->hts/dot_general | solution.py:84
  139.6 18.8 %all-gather = f32[16,1,128]{2,1,0:T(1,128)S(1)} all-gather(f32[2,1,128]{2,1,0:T(1,128)S(1)} %slice_exponential_fusion), channel_id=2, replica_groups=mesh['sp_0'=8,'sp_1'=8,'fs'=4,'tp'=2] {'sp_1'}, dimensions={0}, use_global_device_ids=true | all-gather | bytes 9216 | tf_op jit(solution)/shard_map/all_gather | solution.py:39
  158.5 26.4 %all-gather.10.cloned.1.call-done = f32[16,128,128]{2,1,0:T(8,128)} async-done(((f32[2,128,128]{2,1,0:T(8,128)}), f32[16,128,128]{2,1,0:T(8,128)}) %all-gather.10.cloned.1.call-update) | async-done | bytes 1048592 | tf_op jit(solution)/shard_map/all_gather | solution.py:39
  184.9 2.3 bitcast_add_fusion
  189.3 13.7 %all_gather.23 = f32[8,2,128]{2,1,0:T(2,128)S(1)} all-gather(f32[1,2,128]{2,1,0:T(2,128)S(1)} %get-tuple-element.195), channel_id=1, replica_groups=mesh['sp_0'=8,'sp_1'=8,'fs'=4,'tp'=2] {'sp_0'}, dimensions={0}, use_global_device_ids=true | all-gather | bytes 9216 | tf_op jit(solution)/shard_map/all_gather | solution.py:39
  203.1 25.4 %all-gather.8.cloned.1.call-done = f32[8,2,128,128]{3,2,1,0:T(8,128)} async-done(((f32[1,2,128,128]{3,2,1,0:T(8,128)}), f32[8,2,128,128]{3,2,1,0:T(8,128)}) %all-gather.8.cloned.1.call-update) | async-done | bytes 1048592 | tf_op jit(solution)/shard_map/all_gather | solution.py:39
  228.4 2.6 multiply_reduce_fusion
  231.2 102.4 %all-gather.6.cloned.1.call-done = bf16[8192,512]{1,0:T(8,128)(2,1)} async-done(((bf16[128,512]{1,0:T(8,128)(2,1)}), bf16[8192,512]{1,0:T(8,128)(2,1)}) %all-gather.6.cloned.1.call-update) | async-done | bytes 8388624 | tf_op jit(solution)/shard_map/all_gather | solution.py:24
  334.1 53.6 %conditional.1 = (f32[2,2,128]{2,1,0:T(2,128)S(1)}, f32[2,2,128,128]{3,2,1,0:T(8,128)S(1)}, f32[2,128]{1,0:T(2,128)S(1)}) conditional(s32[]{:T(128)} %bitcast.8, () %tuple.22, (s32[]{:T(128)}, s32[128,1]{0,1:T(1,128)S(1)}, s32[128,8192]{1,0:T(8,128)S(1)}, bf16[8192,512]{1,0:T(8,128)(2,1)}, bf16[2,2,128,64]{2,3,1,0:T(8,128)(2,1)S(1)}) %tuple.88), branch_computations={%region_1.0_spmd, %region_2.5_spmd} | conditional | flops 1657798272 | bytes 109395480 | solution.py:178
  334.8 12.0 %copy.127 = bf16[8192,512]{0,1:T(8,128)(2,1)} copy(bf16[8192,512]{1,0:T(8,128)(2,1)} %get-tuple-element.147) | data formatting | bytes 16777216 | tf_op jit(solution)/shard_map
  346.8 6.0 %fusion.178 = (bf16[8192,256]{0,1:T(8,128)(2,1)}, bf16[8192,256]{0,1:T(8,128)(2,1)}) fusion(bf16[8192,512]{0,1:T(8,128)(2,1)} %copy.127), kind=kLoop, calls=%fused_computation.245 | loop fusion | bytes 16777216 | tf_op jit(solution)/shard_map/split | solution.py:25
  352.7 6.3 %copy.123 = bf16[8192,2,128]{2,0,1:T(8,128)(2,1)} copy(bf16[8192,2,128]{0,2,1:T(8,128)(2,1)} %bitcast.356) | data formatting | bytes 8388608 | tf_op jit(solution)/shard_map/cond/branch_1_fun/reshape | solution.py:116
  359.1 11.2 %fusion.2 = (f32[2,2,128]{2,1,0:T(2,128)S(1)}, f32[2,2,128,8192]{3,2,1,0:T(8,128)}) fusion(pred[128,8192]{1,0:T(8,128)(4,1)S(1)} %broadcast_compare_fusion, bf16[2,2,128,64]{2,3,1,0:T(8,128)(2,1)S(1)} %get-tuple-element.54, bf16[2,2,8192,64]{2,3,1,0:T(8,128)(2,1)} %bitcast.360), kind=kOutput, calls=%fused_computation.3 | convolution fusion | flops 549453312 | bytes 22087680 | tf_op jit(solution)/shard_map/cond/branch_1_fun/hmqd,hmkd->hmqk/dot_general | solution.py:117
  370.3 9.3 %fusion.5 = f32[2,2,128,128]{3,2,1,0:T(8,128)S(1)} fusion(f32[2,2,128,8192]{3,2,1,0:T(8,128)} %get-tuple-element.177, f32[2,2,128]{2,1,0:T(2,128)S(1)} %broadcast_maximum_fusion, pred[128,8192]{1,0:T(8,128)(4,1)S(1)} %broadcast_compare_fusion, bf16[8192,2,128]{2,0,1:T(8,128)(2,1)} %copy.123), kind=kOutput, calls=%fused_computation.6 | convolution fusion | flops 1090519040 | bytes 22284288 | tf_op jit(solution)/shard_map/cond/branch_1_fun/itap,ipn->itan/dot_general | solution.py:124
  379.6 8.1 %fusion.4 = f32[2,2,128]{2,1,0:T(2,128)S(1)} fusion(f32[2,2,128,8192]{3,2,1,0:T(8,128)} %get-tuple-element.177, f32[2,2,128]{2,1,0:T(2,128)S(1)} %broadcast_maximum_fusion, pred[128,8192]{1,0:T(8,128)(4,1)S(1)} %broadcast_compare_fusion), kind=kLoop, calls=%fused_computation.5 | loop fusion | flops 16776704 | bytes 17829888 | tf_op jit(solution)/shard_map/cond/branch_1_fun/reduce_sum | solution.py:123
  389.4 5.1 %all_to_all.10 = bf16[2,128,2048]{2,1,0:T(8,128)(2,1)S(1)} all-to-all(bf16[2,128,2048]{2,1,0:T(8,128)(2,1)S(1)} %broadcast_in_dim.46), channel_id=1, replica_groups=mesh['sp_0'=8,'sp_1'=8,'fs'=4,'tp'=2] {'tp'}, dimensions={0} | all-to-all | bytes 2097152 | tf_op jit(solution)/shard_map/all_to_all | solution.py:51
  394.6 1.1 reduce_sum.51
  (94 shorter events, 13.9 us)
Async XLA Ops:
  7.2 381.5 %copy-start = (bf16[256,2048]{1,0:T(8,128)(2,1)S(1)}, bf16[256,2048]{1,0:T(8,128)(2,1)}, u32[]{:S(2)}) copy-start(bf16[256,2048]{1,0:T(8,128)(2,1)} %param.32) | copy-start | bytes 3145732
  20.7 6.0 %copy-start.3 = (bf16[128,2048]{1,0:T(8,128)(2,1)S(1)}, bf16[128,2048]{1,0:T(8,128)(2,1)}, u32[]{:S(2)}) copy-start(bf16[128,2048]{1,0:T(8,128)(2,1)} %param.19) | copy-start | bytes 1572868
  20.7 6.2 %copy-start.4 = (f32[2,128]{1,0:T(2,128)S(1)}, f32[2,128]{1,0:T(2,128)}, u32[]{:S(2)}) copy-start(f32[2,128]{1,0:T(2,128)} %param.28) | copy-start | bytes 3076
  20.8 94.0 %copy-start.9 = (f32[2048]{0:T(1024)S(1)}, f32[2048]{0:T(1024)}, u32[]{:S(2)}) copy-start(f32[2048]{0:T(1024)} %param.20) | copy-start | bytes 24580
  20.8 94.0 %all-to-all-start = ((bf16[2048,6,256]{0,1,2:T(8,128)(2,1)}), bf16[2048,6,256]{0,1,2:T(8,128)(2,1)}, u32[]{:S(2)}, u32[]{:S(2)}) async-start(bf16[2048,6,256]{0,1,2:T(8,128)(2,1)} %copy.124), calls=%async_computation | async-start | bytes 16777216 | tf_op jit(solution)/shard_map/all_to_all | solution.py:18
  26.5 158.4 %all-gather.10.cloned.1.call-start = ((), (), s32[]{:S(2)}) async-start(), calls=%async_computation.4 | async-start | bytes 1179648 | tf_op jit(solution)/shard_map/all_gather | solution.py:39
  27.0 95.5 %copy-start.5 = (f32[128]{0:T(128)S(1)}, f32[128]{0:T(128)}, u32[]{:S(2)}) copy-start(f32[128]{0:T(128)} %param.29) | copy-start | bytes 1540
  122.6 108.5 %copy-start.6 = (f32[128]{0:T(128)S(1)}, f32[128]{0:T(128)}, u32[]{:S(2)}) copy-start(f32[128]{0:T(128)} %param.31) | copy-start | bytes 1540
  138.7 0.7 copy-start.1
  139.4 89.1 %all-gather.8.cloned.1.call-start = ((), (), s32[]{:S(2)}) async-start(), calls=%async_computation.3 | async-start | bytes 1179648 | tf_op jit(solution)/shard_map/all_gather | solution.py:39
  187.2 146.4 %all-gather.6.cloned.1.call-start = ((), (), s32[]{:S(2)}) async-start(), calls=%async_computation.2 | async-start | bytes 8519680 | tf_op jit(solution)/shard_map/all_gather | solution.py:24
  334.0 54.4 %copy-start.7 = (f32[2]{0:T(128)S(1)}, f32[2]{0:T(128)}, u32[]{:S(2)}) copy-start(f32[2]{0:T(128)} %param.27) | copy-start | bytes 28
  334.1 54.5 %copy-start.8 = (f32[128]{0:T(128)S(1)}, f32[128]{0:T(128)}, u32[]{:S(2)}) copy-start(f32[128]{0:T(128)} %param.30) | copy-start | bytes 1540
  334.1 54.9 %copy-start.2 = (bf16[256,2048]{1,0:T(8,128)(2,1)S(1)}, bf16[256,2048]{1,0:T(8,128)(2,1)}, u32[]{:S(2)}) copy-start(bf16[256,2048]{1,0:T(8,128)(2,1)} %param.33) | copy-start | bytes 3145732
Sparse Core Ops, SparseCore 0:
  139.5 45.3 all-gather.9
  187.3 41.0 all-gather.7
  232.1 101.5 all-gather.5
